TPU v7x, 32 devices: a whole 2x2x4 slice. The times are simulated.
32 devices in a mesh: ep: 8 (over z, y), tp: 4 (over x, core).
Axes of the slice: x: 2, y: 2, z: 4, core: 2. Of those that a mesh axis runs over, the one named last changes fastest.
Arguments:
- tokens: bfloat16 [2048, 2048], P('ep'), may hold values from -6 to 6
- expert_ids: int32 [2048, 2], P('ep'), may hold values from 0 to 7, all different within a row; in each aligned block of 256 rows (0 to 255, 256 to 511, ...) at most 192 rows name the same one
- route_weight: float32 [2048, 2], P('ep'), may hold values from 0.1 to 1
- norm_gain: float32 [2048], replicated, may hold values from 0.1 to 1.9
- expert_gate: bfloat16 [8, 2048, 2048], P('ep', None, 'tp'), may hold values from -4 to 4
- expert_up: bfloat16 [8, 2048, 2048], P('ep', None, 'tp'), may hold values from -4 to 4
- expert_down: bfloat16 [8, 2048, 2048], P('ep', 'tp'), may hold values from -0.03125 to 0.03125
Outputs:
- combined: bfloat16 [2048, 2048], P('ep', 'tp')
Inputs may be any that keep to these rules, and one draw needn't show every extreme that they name: `expert_ids`: each row names 2 different experts. In each aligned block of 256 rows (the rows of one index of ep) no expert is named by more than 192 rows, and in some block one expert is named by exactly 192 rows.
All inputs are finite; a program needn't handle non-finite values.
Results may differ from a plain program's by a relative error of at most 0.012.
Values may be sent and summed in bfloat16 or wider, within the bound.
A program may use at most 128 MiB of HBM per device.

v0:
```python
import jax
import jax.numpy as jnp
from jax import lax
from jax.sharding import PartitionSpec as P

NORM_EPS = 1e-06
CLAMP_LIMIT = 7.0
SWISH_SCALE = 1.702


def normalize(tokens, norm_gain):
    values = tokens.astype(jnp.float32)
    scaled = values * lax.rsqrt(jnp.mean(values * values, axis=-1, keepdims=True) + NORM_EPS)
    return (scaled * norm_gain).astype(jnp.bfloat16)


def activate(gate_sum, up_sum):
    gate_cut = jnp.minimum(gate_sum, CLAMP_LIMIT)
    up_cut = jnp.clip(up_sum, -CLAMP_LIMIT, CLAMP_LIMIT)
    return ((up_cut + 1.0) * gate_cut * jax.nn.sigmoid(SWISH_SCALE * gate_cut)).astype(jnp.bfloat16)


def shards(tokens, expert_ids, route_weight, norm_gain, expert_gate, expert_up, expert_down):
    groups = lax.axis_size("ep")
    tp_count = lax.axis_size("tp")
    member_count = expert_gate.shape[0]
    experts = groups * member_count
    tok_count, model_width = tokens.shape
    top_count = expert_ids.shape[1]
    capacity = min(tok_count, 3 * tok_count * top_count // experts)
    quarter = model_width // tp_count
    normed = normalize(tokens, norm_gain)
    flat_ids = expert_ids.reshape(-1)
    onehot = (flat_ids[:, None] == jnp.arange(experts, dtype=jnp.int32)[None, :]).astype(jnp.int32)
    slot_index = jnp.sum(jnp.cumsum(onehot, axis=0) * onehot, axis=1) - 1
    position = flat_ids * capacity + slot_index
    token_index = jnp.arange(flat_ids.shape[0], dtype=jnp.int32) // top_count
    row_table = jnp.full((experts * capacity,), tok_count, jnp.int32).at[position].set(token_index)
    padded = jnp.concatenate([normed, jnp.zeros((1, model_width), jnp.bfloat16)], axis=0)
    offset = lax.axis_index("tp") * quarter
    source_rows = lax.dynamic_slice_in_dim(padded, offset, quarter, 1)
    send_rows = source_rows[row_table].reshape(groups, member_count, capacity, quarter)
    received = lax.all_to_all(send_rows, "ep", split_axis=0, concat_axis=0, tiled=True)
    slot_count = received.shape[2]
    shard_piece = lax.all_gather(received, "tp", axis=3, tiled=True)
    span_size = shard_piece.shape[3]
    member = 0
    row_block = shard_piece[:, member].reshape(-1, span_size)
    gate_rows = expert_gate[member]
    up_rows = expert_up[member]
    gate_list = [jnp.dot(row_block, gate_rows, preferred_element_type=jnp.float32)]
    up_list = [jnp.dot(row_block, up_rows, preferred_element_type=jnp.float32)]
    gate_sum = jnp.stack(gate_list)
    up_sum = jnp.stack(up_list)
    activated = activate(gate_sum, up_sum)
    member = 0
    weight_rows = expert_down[member]
    product = lax.dot_general(
        weight_rows, activated[member], (((0,), (1,)), ((), ())), preferred_element_type=jnp.float32
    )
    term_list = [product.reshape(quarter * lax.axis_size("tp"), groups, slot_count)]
    summed = lax.psum_scatter(
        jnp.stack(term_list, axis=2).astype(jnp.bfloat16), "tp", scatter_dimension=0, tiled=True
    )
    returned = lax.all_to_all(
        summed.reshape(quarter, experts * capacity), "ep", split_axis=1, concat_axis=1, tiled=True
    )
    picked = jnp.take(returned, position, axis=1).reshape(quarter, tok_count, top_count)
    weighted = jnp.sum(picked.astype(jnp.float32) * route_weight[None, :, :], axis=2)
    return weighted.T.astype(jnp.bfloat16)


def solution(mesh):
    return jax.shard_map(
        shards,
        mesh=mesh,
        in_specs=(
            P("ep", None),
            P("ep", None),
            P("ep", None),
            P(),
            P("ep", None, "tp"),
            P("ep", None, "tp"),
            P("ep", "tp", None),
        ),
        out_specs=P("ep", "tp"),
        check_vma=False,
    )
```

profile of v0, /device:TPU:0, one launch (start us, length us, event | category | flops | bytes accessed | tf_op | source)
XLA Modules:
  0.0 245.8 jit_solution(14064720156240668413)
XLA Ops:
  6.5 1.0 copy.19
  7.5 0.1 eq.26
  7.7 0.1 reshape.111
  7.8 0.7 broadcast_multiply_fusion
  8.5 1.1 reduce-window.6
  9.6 0.2 slice_reduce_fusion
  10.0 0.1 copy.23
  10.1 0.1 mul.76
  10.3 2.5 scatter_custom_fusion
  12.8 1.5 fusion.4
  14.3 1.5 fusion.6
  15.9 5.4 %gather_fusion = bf16[1536,512]{1,0:T(8,128)(2,1)} fusion(bf16[257,512]{1,0:T(8,128)(2,1)S(1)} %pad_dynamic-slice_fusion, s32[2048]{0:T(1024)S(1)} %pad_clamp_fusion), kind=kCustom, calls=%fused_computation | custom fusion | bytes 3151872 | tf_op jit(solution)/shard_map/gather | solution.py:42
  21.3 44.4 %all_to_all.17 = bf16[8,1,192,512]{3,2,1,0:T(8,128)(2,1)} all-to-all(bf16[8,1,192,512]{3,2,1,0:T(8,128)(2,1)} %bitcast.37), channel_id=1, replica_groups=mesh['ep'=8,'tp'=4] {'ep'}, dimensions={0} | all-to-all | bytes 3145728 | tf_op jit(solution)/shard_map/all_to_all | solution.py:43
  65.8 45.5 %all-gather.2.cloned.1.call-done = bf16[8,1,192,2048]{3,2,1,0:T(8,128)(2,1)} async-done(((bf16[8,1,192,512]{3,2,1,0:T(8,128)(2,1)}), bf16[8,1,192,2048]{3,2,1,0:T(8,128)(2,1)}) %all-gather.2.cloned.1.call-update) | async-done | bytes 6291472 | tf_op jit(solution)/shard_map/all_gather | solution.py:45
  111.3 8.5 %convolution_minimum_fusion = f32[1536,512]{1,0:T(8,128)} fusion(bf16[1536,2048]{1,0:T(8,128)(2,1)} %bitcast.43, bf16[1,2048,512]{2,1,0:T(8,128)(2,1)} %param.11), kind=kOutput, calls=%fused_computation.5 | convolution fusion | flops 3222011904 | bytes 11534336 | tf_op jit(solution)/shard_map/dot_general | solution.py:51
  119.8 11.9 %convolution_convert_fusion = bf16[1536,2048]{1,0:T(8,128)(2,1)} fusion(bf16[1,512,2048]{2,1,0:T(8,128)(2,1)S(1)} %copy-done, f32[1536,512]{1,0:T(8,128)} %convolution_minimum_fusion, bf16[1536,2048]{1,0:T(8,128)(2,1)} %bitcast.44, bf16[1,2048,512]{2,1,0:T(8,128)(2,1)} %param.12), kind=kOutput, calls=%fused_computation.3 | convolution fusion | flops 6452674560 | bytes 19922944 | tf_op jit(solution)/shard_map/dot_general | solution.py:58
  131.7 58.0 %reduce-scatter.2.cloned.1.call-done = bf16[512,8,1,192]{0,3,1,2:T(8,128)(2,1)} async-done(((bf16[2048,8,1,192]{0,3,1,2:T(8,128)(2,1)}), bf16[512,8,1,192]{0,3,1,2:T(8,128)(2,1)}) %reduce-scatter.2.cloned.1.call-update) | async-done | bytes 1572880 | tf_op jit(solution)/shard_map/reduce_scatter | solution.py:62
  189.7 5.5 %all-to-all-start.1 = ((bf16[512,8,192]{0,2,1:T(8,128)(2,1)}), bf16[512,8,192]{0,2,1:T(8,128)(2,1)}, u32[]{:S(2)}, u32[]{:S(2)}) async-start(bf16[512,8,192]{0,2,1:T(8,128)(2,1)} %bitcast.39), calls=%async_computation.2 | async-start | bytes 3145728 | tf_op jit(solution)/shard_map/all_to_all | solution.py:65
  195.2 0.1 sub.15
  195.5 0.2 copy.22
  195.8 36.3 %all-to-all-done.1 = bf16[512,8,192]{0,2,1:T(8,128)(2,1)} async-done(((bf16[512,8,192]{0,2,1:T(8,128)(2,1)}), bf16[512,8,192]{0,2,1:T(8,128)(2,1)}, u32[]{:S(2)}, u32[]{:S(2)}) %all-to-all-start.1) | async-done | bytes 1572896 | tf_op jit(solution)/shard_map/all_to_all | solution.py:65
  232.2 3.6 %gather_fusion.1 = bf16[512,512]{1,0:T(8,128)(2,1)S(1)} fusion(bf16[512,1536]{0,1:T(8,128)(2,1)} %bitcast.13, s32[1024]{0:T(1024)S(1)} %pad_clamp_fusion.1), kind=kCustom, calls=%fused_computation.1 | custom fusion | bytes 1050624 | tf_op jit(solution)/shard_map/jit(_take)/gather | solution.py:68
  235.8 0.2 gather.11
  236.0 2.9 %multiply_reduce_fusion = bf16[512,256]{0,1:T(8,128)(2,1)} fusion(bf16[512,256,2]{0,2,1:T(2,128)(2,1)S(1)} %gather.11, pred[256,2]{1,0:T(8,128)(4,1)S(1)} %copy.22, f32[256,2]{1,0:T(8,128)S(1)} %copy.25), kind=kLoop, calls=%fused_computation.19 | loop fusion | flops 917504 | bytes 788992 | tf_op jit(solution)/shard_map/reduce_sum | solution.py:69
  (25 shorter events, 0.5 us)
Async XLA Ops:
  6.5 113.3 %copy-start = (bf16[1,512,2048]{2,1,0:T(8,128)(2,1)S(1)}, bf16[1,512,2048]{2,1,0:T(8,128)(2,1)}, u32[]{:S(2)}) copy-start(bf16[1,512,2048]{2,1,0:T(8,128)(2,1)} %param.13) | copy-start | bytes 6291460
  6.5 104.7 %all-gather.2.cloned.1.call-start = ((), (), s32[]{:S(2)}) async-start(), calls=%async_computation.3 | async-start | bytes 7864320 | tf_op jit(solution)/shard_map/all_gather | solution.py:45
  65.8 124.0 %reduce-scatter.2.cloned.1.call-start = ((), (), s32[]{:S(2)}) async-start(), calls=%async_computation.4 | async-start | bytes 7864320 | tf_op jit(solution)/shard_map/reduce_scatter | solution.py:62
  131.7 63.8 %copy-start.1 = (s32[256,2]{0,1:T(2,128)S(1)}, s32[256,2]{0,1:T(2,128)}, u32[]{:S(2)}) copy-start(s32[256,2]{0,1:T(2,128)} %param.8) | copy-start | bytes 6148
  131.7 64.0 %copy-start.2 = (f32[256,2]{0,1:T(2,128)S(1)}, f32[256,2]{0,1:T(2,128)}, u32[]{:S(2)}) copy-start(f32[256,2]{0,1:T(2,128)} %param.9) | copy-start | bytes 6148
  189.7 42.4 %all-to-all-start.1 = ((bf16[512,8,192]{0,2,1:T(8,128)(2,1)}), bf16[512,8,192]{0,2,1:T(8,128)(2,1)}, u32[]{:S(2)}, u32[]{:S(2)}) async-start(bf16[512,8,192]{0,2,1:T(8,128)(2,1)} %bitcast.39), calls=%async_computation.2 | async-start | bytes 3145728 | tf_op jit(solution)/shard_map/all_to_all | solution.py:65
Sparse Core Ops, SparseCore 0:
  65.9 45.3 all-gather.1
  131.8 57.8 reduce-scatter.1
where the time goes:
time: 246 us
  waiting for transfers between devices  140 us (57%)
  blocking collectives  44.4 us (18%)
  matrix products  20.4 us (8%)
  local copies, waits for them, and re-layouts  14 us (6%)
  between operations  13.6 us (6%)
  other arithmetic  8.01 us (3%)
  starting transfers between devices  5.56 us (2%)
    reduce_scatter x1, waiting for transfers between devices, shards(): lax.psum_scatter(jnp.stack(term_list, axis=2).astype(jnp.bfloat16), 'tp',...  58 us
    all_gather x1, waiting for transfers between devices, shards(): shard_piece = lax.all_gather(received, 'tp', axis=3, tiled=True)  45.5 us
    all_to_all x1, blocking collectives, shards(): lax.all_to_all(send_rows, 'ep', split_axis=0, concat_axis=0, tiled=True)  44.4 us
    all_to_all x1, waiting for transfers between devices, shards(): lax.all_to_all(summed.reshape(quarter, experts * capacity), 'ep', split_a...  36.3 us
    dot_general x1, matrix products, shards(): lax.dot_general(weight_rows, activated[member], (((0,), (1,)), ((), ())),...  11.9 us
    dot_general x1, matrix products, shards(): jnp.dot(row_block, gate_rows, preferred_element_type=jnp.float32)  8.52 us
    all_to_all x1, starting transfers between devices, shards(): lax.all_to_all(summed.reshape(quarter, experts * capacity), 'ep', split_a...  5.51 us
    gather x1, local copies, waits for them, and re-layouts, shards(): source_rows[row_table].reshape(groups, member_count, capacity, quarter)  5.43 us
  transfers between devices with their start and end apart: 3, of which 3 were waited for; matrix products, arithmetic and copies ran while one was open for 0% of the time, Pallas kernels for 0%

commit v1 on v0

--- a/solution.py
+++ b/solution.py
@@ -42,7 +42,8 @@
     send_rows = source_rows[row_table].reshape(groups, member_count, capacity, quarter)
     received = lax.all_to_all(send_rows, "ep", split_axis=0, concat_axis=0, tiled=True)
     slot_count = received.shape[2]
-    shard_piece = lax.all_gather(received, "tp", axis=3, tiled=True)
+    shards_2 = lax.all_gather(received, "tp")
+    shard_piece = jnp.concatenate(shards_2, axis=3)
     span_size = shard_piece.shape[3]
     member = 0
     row_block = shard_piece[:, member].reshape(-1, span_size)

time: 246 us -> 261 us (1.061)
  local copies, waits for them, and re-layouts: 14 us -> 32.6 us
  matrix products: 20.4 us -> 17.1 us
    reshape x0 -> x1, local copies, waits for them, and re-layouts: none -> 10.3 us  [shards(): shard_piece = jnp.concatenate(shards_2, axis=3)]
    unnamed x8 -> x13, local copies, waits for them, and re-layouts: 1.11 us -> 9.38 us
    dot_general x1, matrix products: 8.52 us -> 5.18 us  [shards(): jnp.dot(row_block, gate_rows, preferred_element_type=jnp.float32)]
where the time goes in v1:
time: 261 us
  waiting for transfers between devices  140 us (54%)
  blocking collectives  44.4 us (17%)
  local copies, waits for them, and re-layouts  32.6 us (12%)
  matrix products  17.1 us (7%)
  between operations  13.6 us (5%)
  other arithmetic  7.98 us (3%)
  starting transfers between devices  5.77 us (2%)
    reduce_scatter x1, waiting for transfers between devices, shards(): lax.psum_scatter(jnp.stack(term_list, axis=2).astype(jnp.bfloat16), 'tp',...  58 us
    all_gather x1, waiting for transfers between devices, shards(): shards_2 = lax.all_gather(received, 'tp')  45.3 us
    all_to_all x1, blocking collectives, shards(): lax.all_to_all(send_rows, 'ep', split_axis=0, concat_axis=0, tiled=True)  44.4 us
    all_to_all x1, waiting for transfers between devices, shards(): lax.all_to_all(summed.reshape(quarter, experts * capacity), 'ep', split_a...  36.3 us
    dot_general x1, matrix products, shards(): lax.dot_general(weight_rows, activated[member], (((0,), (1,)), ((), ())),...  11.9 us
    reshape x1, local copies, waits for them, and re-layouts, shards(): shard_piece = jnp.concatenate(shards_2, axis=3)  10.3 us
    unnamed x13, local copies, waits for them, and re-layouts  9.38 us
    all_to_all x1, starting transfers between devices, shards(): lax.all_to_all(summed.reshape(quarter, experts * capacity), 'ep', split_a...  5.54 us
  transfers between devices with their start and end apart: 3, of which 3 were waited for; matrix products, arithmetic and copies ran while one was open for 0% of the time, Pallas kernels for 0%

profile of v1, /device:TPU:0, one launch (start us, length us, event | category | flops | bytes accessed | tf_op | source)
XLA Modules:
  0.0 261.1 jit_solution(1816204147233620051)
XLA Ops:
  6.5 1.0 copy.25
  7.8 0.7 broadcast_multiply_fusion
  8.5 1.1 reduce-window.6
  9.6 0.2 slice_reduce_fusion
  10.1 0.1 mul.76
  10.3 2.5 scatter_custom_fusion
  12.8 1.5 fusion.4
  14.3 1.5 fusion.6
  15.9 5.4 %gather_fusion = bf16[1536,512]{1,0:T(8,128)(2,1)} fusion(bf16[257,512]{1,0:T(8,128)(2,1)S(1)} %pad_dynamic-slice_fusion, s32[2048]{0:T(1024)S(1)} %pad_clamp_fusion), kind=kCustom, calls=%fused_computation | custom fusion | bytes 3151872 | tf_op jit(solution)/shard_map/gather | solution.py:42
  21.3 44.4 %all_to_all.17 = bf16[8,1,192,512]{3,2,1,0:T(8,128)(2,1)} all-to-all(bf16[8,1,192,512]{3,2,1,0:T(8,128)(2,1)} %bitcast.47), channel_id=1, replica_groups=mesh['ep'=8,'tp'=4] {'ep'}, dimensions={0} | all-to-all | bytes 3145728 | tf_op jit(solution)/shard_map/all_to_all | solution.py:43
  65.8 0.2 reduce-scatter.2.cloned.1.call-start
  66.0 45.3 %all-gather.3.cloned.1.call-done = bf16[32,1,192,512]{3,2,1,0:T(8,128)(2,1)} async-done(((bf16[8,1,192,512]{3,2,1,0:T(8,128)(2,1)}), bf16[32,1,192,512]{3,2,1,0:T(8,128)(2,1)}) %all-gather.3.cloned.1.call-update) | async-done | bytes 6291472 | tf_op jit(solution)/shard_map/all_gather | solution.py:45
  111.3 10.3 %copy.31 = bf16[8,1,192,4,512]{4,3,2,0,1:T(4,128)(2,1)} copy(bf16[8,1,192,4,512]{4,2,0,3,1:T(8,128)(2,1)} %bitcast.43) | data formatting | bytes 12582912 | tf_op jit(solution)/shard_map/reshape | solution.py:46
  121.6 5.6 %copy.33 = bf16[192,8,4,512]{3,1,2,0:T(8,128)(2,1)S(1)} copy(bf16[192,8,4,512]{3,2,1,0:T(4,128)(2,1)} %bitcast.42) | data formatting | bytes 12582912
  127.2 2.6 %copy-done.1 = bf16[192,8,4,512]{3,1,2,0:T(8,128)(2,1)} copy-done((bf16[192,8,4,512]{3,1,2,0:T(8,128)(2,1)}, bf16[192,8,4,512]{3,1,2,0:T(8,128)(2,1)S(1)}, u32[]{:S(2)}) %copy-start.1) | copy-done | bytes 6291480
  129.9 5.2 %convolution_minimum_fusion = f32[1536,512]{1,0:T(8,128)} fusion(bf16[1536,2048]{1,0:T(8,128)(2,1)S(1)} %bitcast.45, bf16[1,2048,512]{2,1,0:T(8,128)(2,1)S(1)} %copy-done.4), kind=kOutput, calls=%fused_computation.5 | convolution fusion | flops 3222011904 | bytes 11534336 | tf_op jit(solution)/shard_map/dot_general | solution.py:52
  135.0 11.9 %convolution_convert_fusion = bf16[1536,2048]{1,0:T(8,128)(2,1)} fusion(bf16[1,512,2048]{2,1,0:T(8,128)(2,1)S(1)} %copy-done, f32[1536,512]{1,0:T(8,128)} %convolution_minimum_fusion, bf16[1536,2048]{1,0:T(8,128)(2,1)} %bitcast.46, bf16[1,2048,512]{2,1,0:T(8,128)(2,1)} %param.12), kind=kOutput, calls=%fused_computation.3 | convolution fusion | flops 6452674560 | bytes 19922944 | tf_op jit(solution)/shard_map/dot_general | solution.py:59
  147.0 58.0 %reduce-scatter.2.cloned.1.call-done = bf16[512,8,1,192]{0,3,1,2:T(8,128)(2,1)} async-done(((bf16[2048,8,1,192]{0,3,1,2:T(8,128)(2,1)}), bf16[512,8,1,192]{0,3,1,2:T(8,128)(2,1)}) %reduce-scatter.2.cloned.1.call-update) | async-done | bytes 1572880 | tf_op jit(solution)/shard_map/reduce_scatter | solution.py:63
  205.0 5.5 %all-to-all-start.1 = ((bf16[512,8,192]{0,2,1:T(8,128)(2,1)}), bf16[512,8,192]{0,2,1:T(8,128)(2,1)}, u32[]{:S(2)}, u32[]{:S(2)}) async-start(bf16[512,8,192]{0,2,1:T(8,128)(2,1)} %bitcast.49), calls=%async_computation.2 | async-start | bytes 3145728 | tf_op jit(solution)/shard_map/all_to_all | solution.py:66
  210.8 0.2 copy.28
  211.2 36.3 %all-to-all-done.1 = bf16[512,8,192]{0,2,1:T(8,128)(2,1)} async-done(((bf16[512,8,192]{0,2,1:T(8,128)(2,1)}), bf16[512,8,192]{0,2,1:T(8,128)(2,1)}, u32[]{:S(2)}, u32[]{:S(2)}) %all-to-all-start.1) | async-done | bytes 1572896 | tf_op jit(solution)/shard_map/all_to_all | solution.py:66
  247.5 3.6 %gather_fusion.1 = bf16[512,512]{1,0:T(8,128)(2,1)S(1)} fusion(bf16[512,1536]{0,1:T(8,128)(2,1)} %bitcast.14, s32[1024]{0:T(1024)S(1)} %pad_clamp_fusion.1), kind=kCustom, calls=%fused_computation.1 | custom fusion | bytes 1050624 | tf_op jit(solution)/shard_map/jit(_take)/gather | solution.py:69
  251.1 0.2 gather.11
  251.3 2.9 %multiply_reduce_fusion = bf16[512,256]{0,1:T(8,128)(2,1)} fusion(bf16[512,256,2]{0,2,1:T(2,128)(2,1)S(1)} %gather.11, pred[256,2]{1,0:T(8,128)(4,1)S(1)} %copy.28, f32[256,2]{1,0:T(8,128)S(1)} %copy.32), kind=kLoop, calls=%fused_computation.19 | loop fusion | flops 917504 | bytes 788992 | tf_op jit(solution)/shard_map/reduce_sum | solution.py:70
  (31 shorter events, 1.0 us)
Async XLA Ops:
  6.5 128.5 %copy-start = (bf16[1,512,2048]{2,1,0:T(8,128)(2,1)S(1)}, bf16[1,512,2048]{2,1,0:T(8,128)(2,1)}, u32[]{:S(2)}) copy-start(bf16[1,512,2048]{2,1,0:T(8,128)(2,1)} %param.13) | copy-start | bytes 6291460
  6.5 104.7 %all-gather.3.cloned.1.call-start = ((), (), s32[]{:S(2)}) async-start(), calls=%async_computation.4 | async-start | bytes 7864320 | tf_op jit(solution)/shard_map/all_gather | solution.py:45
  65.8 139.3 %reduce-scatter.2.cloned.1.call-start = ((), (), s32[]{:S(2)}) async-start(), calls=%async_computation.3 | async-start | bytes 7864320 | tf_op jit(solution)/shard_map/reduce_scatter | solution.py:63
  121.6 8.3 %copy-start.4 = (bf16[1,2048,512]{2,1,0:T(8,128)(2,1)S(1)}, bf16[1,2048,512]{2,1,0:T(8,128)(2,1)}, u32[]{:S(2)}) copy-start(bf16[1,2048,512]{2,1,0:T(8,128)(2,1)} %param.11) | copy-start | bytes 6291460
  127.2 2.7 %copy-start.1 = (bf16[192,8,4,512]{3,1,2,0:T(8,128)(2,1)}, bf16[192,8,4,512]{3,1,2,0:T(8,128)(2,1)S(1)}, u32[]{:S(2)}) copy-start(bf16[192,8,4,512]{3,1,2,0:T(8,128)(2,1)S(1)} %copy.33) | copy-start | bytes 18874372
  147.0 63.8 %copy-start.2 = (s32[256,2]{0,1:T(2,128)S(1)}, s32[256,2]{0,1:T(2,128)}, u32[]{:S(2)}) copy-start(s32[256,2]{0,1:T(2,128)} %param.8) | copy-start | bytes 6148
  147.0 64.0 %copy-start.3 = (f32[256,2]{0,1:T(2,128)S(1)}, f32[256,2]{0,1:T(2,128)}, u32[]{:S(2)}) copy-start(f32[256,2]{0,1:T(2,128)} %param.9) | copy-start | bytes 6148
  205.0 42.5 %all-to-all-start.1 = ((bf16[512,8,192]{0,2,1:T(8,128)(2,1)}), bf16[512,8,192]{0,2,1:T(8,128)(2,1)}, u32[]{:S(2)}, u32[]{:S(2)}) async-start(bf16[512,8,192]{0,2,1:T(8,128)(2,1)} %bitcast.49), calls=%async_computation.2 | async-start | bytes 3145728 | tf_op jit(solution)/shard_map/all_to_all | solution.py:66
Sparse Core Ops, SparseCore 0:
  65.9 45.3 all-gather.2
  147.1 57.8 reduce-scatter.1
